TPU v7x, 32 devices: a whole 2x2x4 slice. The times are simulated.
32 devices in a mesh: ep: 4 (over y, x), tp: 8 (over z, core).
Axes of the slice: x: 2, y: 2, z: 4, core: 2. Of those that a mesh axis runs over, the one named last changes fastest.
Arguments:
- tokens: bfloat16 [128, 4096], P('ep', 'tp'), may hold values from -16 to 16
- routing: int32 [128, 4], P('ep'), may hold values from 0 to 7, all different within a row; in each aligned block of 32 rows (0 to 31, 32 to 63, ...) at most 32 rows name the same one
- gate_weights: float32 [128, 4], P('ep'), may hold values from 0.1 to 1
- w_gate: bfloat16 [8, 1024, 4096], P('ep', 'tp'), may hold values from -0.09375 to 0.09375
- w_up: bfloat16 [8, 1024, 4096], P('ep', 'tp'), may hold values from -0.09375 to 0.09375
- w_down: bfloat16 [8, 1024, 4096], P('ep', None, 'tp'), may hold values from -2 to 2
- out_gain: float32 [4096], P('tp'), may hold values from 0.1 to 1.9
Outputs:
- mixed: bfloat16 [128, 4096], P('ep', 'tp')
Inputs may be any that keep to these rules, and one draw needn't show every extreme that they name: `routing`: in each aligned block of 32 rows (the tokens of one index of ep) no expert is named by more than 32 entries, and in every draw some expert is named by exactly 32 entries of some block. The 4 entries of a row differ.
All inputs are finite; a program needn't handle non-finite values.
Results may differ from a plain program's by a relative error of at most 0.0057.
Values may be sent and summed in bfloat16 or wider, within the bound.
A program may use at most 64 MiB of HBM per device.

v0:
```python
import jax
import jax.numpy as jnp
from jax import lax
from jax.sharding import PartitionSpec as P

D = 4096
TOPK = 4
EXP_DEV = 2
norm_eps = 1e-05


def body(tokens, routing, gate_weights, w_gate, w_up, w_down, out_gain):
    ep_count = lax.axis_size("ep")
    tok_rows = tokens.shape[0]
    width_part = tokens.shape[1]
    experts = EXP_DEV * ep_count
    slot_count = 2 * tok_rows * TOPK // experts
    span_rows = ep_count * slot_count
    total_slots = EXP_DEV * span_rows
    flat_route = routing.reshape(-1)
    expert_ids = jnp.arange(experts, dtype=jnp.int32)
    hit_table = (flat_route[:, None] == expert_ids[None, :]).astype(jnp.int32)
    running = jnp.cumsum(hit_table, axis=0) - hit_table
    slot_rank = jnp.sum(running * hit_table, axis=1)
    slot_target = flat_route % EXP_DEV * span_rows + flat_route // EXP_DEV * slot_count + slot_rank
    entry_targets = slot_target.reshape(tok_rows, TOPK)
    slot_ids = jnp.arange(total_slots, dtype=jnp.int32)
    select_table = jnp.any(entry_targets[None, :, :] == slot_ids[:, None, None], axis=2).astype(
        jnp.bfloat16
    )
    outgoing = jnp.dot(select_table, tokens, preferred_element_type=jnp.float32).astype(
        jnp.bfloat16
    )
    outgoing = outgoing.reshape(EXP_DEV, ep_count, slot_count, width_part)
    arrived = lax.all_to_all(outgoing, "ep", split_axis=1, concat_axis=1, tiled=True).reshape(
        EXP_DEV, span_rows, width_part
    )
    piece_cols = lax.all_gather(arrived, "tp", axis=2, tiled=True)
    gate_sum = jnp.einsum("efn,esn->efs", w_gate, piece_cols, preferred_element_type=jnp.float32)
    up_sum = jnp.einsum("efn,esn->efs", w_up, piece_cols, preferred_element_type=jnp.float32)
    square_sum = jnp.einsum(
        "esn,esn->es", piece_cols, piece_cols, preferred_element_type=jnp.float32
    )
    row_scale = lax.rsqrt(square_sum / D + norm_eps)[:, None, :]
    hidden = (jax.nn.silu(gate_sum * row_scale) * (up_sum * row_scale)).astype(jnp.bfloat16)
    out_part = w_down.shape[2]
    expert_out = jnp.einsum(
        "ens,end->esd",
        lax.all_gather(hidden, "tp", axis=1, tiled=True),
        w_down,
        preferred_element_type=jnp.float32,
    ).astype(jnp.bfloat16)
    returned = lax.all_to_all(
        expert_out.reshape(EXP_DEV, ep_count, slot_count, out_part),
        "ep",
        split_axis=1,
        concat_axis=1,
        tiled=True,
    )
    returned = returned.reshape(total_slots, out_part)
    chosen = returned[slot_target].astype(jnp.float32).reshape(tok_rows, TOPK, out_part)
    combined = jnp.sum(chosen * gate_weights[:, :, None], axis=1)
    square_total = lax.psum(jnp.sum(combined * combined, axis=1), "tp")
    final_scale = lax.rsqrt(square_total / D + norm_eps)
    return (combined * final_scale[:, None] * out_gain[None, :]).astype(jnp.bfloat16)


def solution(mesh):
    placed = (
        P("ep", "tp"),
        P("ep", None),
        P("ep", None),
        P("ep", "tp", None),
        P("ep", "tp", None),
        P("ep", None, "tp"),
        P("tp"),
    )
    return jax.shard_map(body, mesh=mesh, in_specs=placed, out_specs=P("ep", "tp"), check_vma=False)
```

profile of v0, /device:TPU:0, one launch (start us, length us, event | category | flops | bytes accessed | tf_op | source)
XLA Modules:
  0.0 102.4 jit_solution(12375172439346588443)
XLA Ops:
  6.5 0.0 copy-start
  6.5 0.0 all-gather.2.cloned.1.call-start
  6.5 0.9 copy.33
  7.5 0.1 eq.30
  7.6 0.1 fusion.6
  7.7 0.2 reduce_window_sum.11
  7.8 0.2 select_reduce_fusion
  8.0 0.1 reduce_sum.32
  8.1 0.1 copy.38
  8.2 0.1 fusion.5
  8.3 1.0 convolution_convert_fusion
  9.4 10.7 %all_to_all.10 = bf16[2,4,32,512]{3,2,0,1:T(8,128)(2,1)S(1)} all-to-all(bf16[2,4,32,512]{3,2,0,1:T(8,128)(2,1)S(1)} %copy.39), channel_id=1, replica_groups=mesh['ep'=4,'tp'=8] {'ep'}, dimensions={1} | all-to-all | bytes 524288 | tf_op jit(solution)/shard_map/all_to_all | solution.py:35
  20.1 0.7 copy.40
  20.8 0.0 all-gather.2.cloned.1.call-update
  20.9 0.1 reshape.182
  21.0 28.9 %all-gather.2.cloned.1.call-done = bf16[2,128,4096]{2,1,0:T(8,128)(2,1)} async-done(((bf16[2,128,512]{2,1,0:T(8,128)(2,1)}), bf16[2,128,4096]{2,1,0:T(8,128)(2,1)}) %all-gather.2.cloned.1.call-update) | async-done | bytes 2097168 | tf_op jit(solution)/shard_map/all_gather | solution.py:38
  49.9 0.0 copy-start.1
  49.9 2.2 %fusion = f32[2,128]{1,0:T(2,128)S(1)} fusion(bf16[2,128,4096]{2,1,0:T(8,128)(2,1)} %all-gather.2.cloned.1.call-done), kind=kLoop, calls=%fused_computation.2 | loop fusion | flops 3145472 | bytes 2098176 | tf_op jit(solution)/shard_map/esn,esn->es/dot_general | solution.py:41
  52.1 0.0 copy-done.1
  52.1 0.0 copy-start.4
  52.2 2.5 %fusion.3 = f32[2,128,128]{1,2,0:T(8,128)S(1)} fusion(bf16[2,128,4096]{2,1,0:T(8,128)(2,1)S(1)} %copy-done.1, bf16[2,128,4096]{2,1,0:T(8,128)(2,1)} %param.10, f32[2,128]{1,0:T(2,128)S(1)} %add_rsqrt_fusion), kind=kOutput, calls=%fused_computation.9 | convolution fusion | flops 268468224 | bytes 4326400 | tf_op jit(solution)/shard_map/efn,esn->efs/dot_general | solution.py:39
  54.6 0.0 copy-done.4
  54.6 0.7 fusion.4
  55.3 13.9 %all_gather.7 = bf16[2,1024,128]{1,2,0:T(8,128)(2,1)S(1)} all-gather(bf16[2,128,128]{1,2,0:T(8,128)(2,1)S(1)} %fusion.4), channel_id=1, replica_groups=mesh['ep'=4,'tp'=8] {'tp'}, dimensions={1}, use_global_device_ids=true | all-gather | bytes 589824 | tf_op jit(solution)/shard_map/all_gather | solution.py:49
  69.2 0.0 copy-done
  69.2 0.0 copy-start.2
  69.2 0.4 convolution_convert_fusion.1
  69.7 0.0 copy-start.3
  69.7 0.7 copy.41
  70.4 3.6 %all-to-all-start.1 = ((bf16[2,4,32,512]{3,2,0,1:T(8,128)(2,1)}), bf16[2,4,32,512]{3,2,0,1:T(8,128)(2,1)S(1)}, u32[]{:S(2)}, u32[]{:S(2)}) async-start(bf16[2,4,32,512]{3,2,0,1:T(8,128)(2,1)} %copy.41), calls=%async_computation.1 | async-start | bytes 524288 | tf_op jit(solution)/shard_map/all_to_all | solution.py:53
  74.1 0.0 copy-done.2
  74.1 0.1 copy.44
  74.2 5.8 %all-to-all-done.1 = bf16[2,4,32,512]{3,2,0,1:T(8,128)(2,1)S(1)} async-done(((bf16[2,4,32,512]{3,2,0,1:T(8,128)(2,1)}), bf16[2,4,32,512]{3,2,0,1:T(8,128)(2,1)S(1)}, u32[]{:S(2)}, u32[]{:S(2)}) %all-to-all-start.1) | async-done | bytes 262176 | tf_op jit(solution)/shard_map/all_to_all | solution.py:53
  80.0 0.8 gather_fusion
  80.8 0.1 reshape.183
  80.9 0.2 multiply_reduce_fusion
  81.1 0.1 multiply_reduce_fusion.1
  81.2 13.6 %psum.7 = f32[32]{0:T(128)S(1)} all-reduce(f32[32]{0:T(128)S(1)} %multiply_reduce_fusion.1), channel_id=1, replica_groups=mesh['ep'=4,'tp'=8] {'tp'}, use_global_device_ids=true, to_apply=%region_5.6 | all-reduce | flops 32 | bytes 256 | tf_op jit(solution)/shard_map/psum | solution.py:63
  94.8 0.0 copy-done.3
  94.8 0.7 multiply_convert_fusion
  (7 shorter events, 0.1 us)
Async XLA Ops:
  6.5 62.7 %copy-start = (bf16[2,1024,512]{2,1,0:T(8,128)(2,1)S(1)}, bf16[2,1024,512]{2,1,0:T(8,128)(2,1)}, u32[]{:S(2)}) copy-start(bf16[2,1024,512]{2,1,0:T(8,128)(2,1)} %param.12) | copy-start | bytes 6291460
  6.5 43.4 %all-gather.2.cloned.1.call-start = ((), (), s32[]{:S(2)}) async-start(), calls=%async_computation.2 | async-start | bytes 2359296 | tf_op jit(solution)/shard_map/all_gather | solution.py:38
  49.9 2.2 %copy-start.1 = (bf16[2,128,4096]{2,1,0:T(8,128)(2,1)S(1)}, bf16[2,128,4096]{2,1,0:T(8,128)(2,1)}, u32[]{:S(2)}) copy-start(bf16[2,128,4096]{2,1,0:T(8,128)(2,1)} %all-gather.2.cloned.1.call-done) | copy-start | bytes 6291460
  52.1 2.5 %copy-start.4 = (bf16[2,128,4096]{2,1,0:T(8,128)(2,1)S(1)}, bf16[2,128,4096]{2,1,0:T(8,128)(2,1)}, u32[]{:S(2)}) copy-start(bf16[2,128,4096]{2,1,0:T(8,128)(2,1)} %param.11) | copy-start | bytes 6291460
  69.2 4.8 %copy-start.2 = (f32[32,4]{0,1:T(4,128)S(1)}, f32[32,4]{0,1:T(4,128)}, u32[]{:S(2)}) copy-start(f32[32,4]{0,1:T(4,128)} %param.9) | copy-start | bytes 1540
  69.7 25.2 %copy-start.3 = (f32[512]{0:T(512)S(1)}, f32[512]{0:T(512)}, u32[]{:S(2)}) copy-start(f32[512]{0:T(512)} %param.13) | copy-start | bytes 6148
  70.4 9.5 %all-to-all-start.1 = ((bf16[2,4,32,512]{3,2,0,1:T(8,128)(2,1)}), bf16[2,4,32,512]{3,2,0,1:T(8,128)(2,1)S(1)}, u32[]{:S(2)}, u32[]{:S(2)}) async-start(bf16[2,4,32,512]{3,2,0,1:T(8,128)(2,1)} %copy.41), calls=%async_computation.1 | async-start | bytes 524288 | tf_op jit(solution)/shard_map/all_to_all | solution.py:53
Sparse Core Ops, SparseCore 0:
  21.0 28.8 all-gather.1
where the time goes:
time: 103 us; the launch traced here: 102 us
  blocking collectives  38.2 us (37%)
  waiting for transfers between devices  34.7 us (34%)
  between operations  13.5 us (13%)
  matrix products  4.63 us (4%)
  other arithmetic  3.86 us (4%)
  local copies, waits for them, and re-layouts  3.84 us (4%)
  starting transfers between devices  3.65 us (4%)
    all_gather x1, waiting for transfers between devices, body(): piece_cols = lax.all_gather(arrived, 'tp', axis=2, tiled=True)  28.9 us
    all_gather x1, blocking collectives, body(): lax.all_gather(hidden, 'tp', axis=1, tiled=True)  13.9 us
    psum x1, blocking collectives, body(): square_total = lax.psum(jnp.sum(combined * combined, axis=1), 'tp')  13.6 us
    all_to_all x1, blocking collectives, body(): lax.all_to_all(outgoing, 'ep', split_axis=1, concat_axis=1, tiled=True)  10.7 us
    all_to_all x1, waiting for transfers between devices, body(): lax.all_to_all(expert_out.reshape(EXP_DEV, ep_count, slot_count, out_part...  5.77 us
    all_to_all x1, starting transfers between devices, body(): lax.all_to_all(expert_out.reshape(EXP_DEV, ep_count, slot_count, out_part...  3.65 us
    dot_general x1, matrix products, body(): jnp.einsum('efn,esn->efs', w_gate, piece_cols, preferred_element_type=jnp...  2.45 us
    dot_general x1, other arithmetic, body(): jnp.einsum('esn,esn->es', piece_cols, piece_cols, preferred_element_type=...  2.23 us
  transfers between devices with their start and end apart: 2, of which 2 were waited for; matrix products, arithmetic and copies ran while one was open for 0% of the time, Pallas kernels for 0%

commit v1 on v0

--- a/solution.py
+++ b/solution.py
@@ -44,11 +44,34 @@
     row_scale = lax.rsqrt(square_sum / D + norm_eps)[:, None, :]
     hidden = (jax.nn.silu(gate_sum * row_scale) * (up_sum * row_scale)).astype(jnp.bfloat16)
     out_part = w_down.shape[2]
-    expert_out = jnp.einsum(
-        "ens,end->esd",
-        lax.all_gather(hidden, "tp", axis=1, tiled=True),
-        w_down,
-        preferred_element_type=jnp.float32,
+
+    def start_patches(local_array, vector):
+        r2 = lax.axis_index("tp")
+        inter = lax.axis_size("tp")
+        y_new, local_part, h_now = (inter, r2, local_array.shape[1])
+        by_rank = tuple(((num, (num + 1) % y_new) for num in range(y_new)))
+        all_rows = tuple(((num, (num - 1) % y_new) for num in range(y_new)))
+        low = upper = local_array
+        a_next = y_new // 2
+        x_new = vector(local_array, local_part * h_now)
+        for h in [*range(1, a_next + 1)]:
+            low = lax.ppermute(low, "tp", by_rank)
+            if h < y_new - a_next:
+                upper = lax.ppermute(upper, "tp", all_rows)
+                after = vector(upper, (local_part + h) % y_new * h_now)
+                x_new = x_new + after
+            field_out = vector(low, (local_part - h) % y_new * h_now)
+            x_new = x_new + field_out
+        return x_new
+
+    expert_out = start_patches(
+        hidden,
+        vector=lambda own_block, start: jnp.einsum(
+            "ens,end->esd",
+            own_block,
+            lax.dynamic_slice_in_dim(w_down, start, own_block.shape[1], axis=1),
+            preferred_element_type=jnp.float32,
+        ),
     ).astype(jnp.bfloat16)
     returned = lax.all_to_all(
         expert_out.reshape(EXP_DEV, ep_count, slot_count, out_part),

time: 103 us -> 110 us (1.068)
  blocking collectives: 38.2 us -> 24.3 us
  starting transfers between devices: 3.65 us -> 14.4 us
  waiting for transfers between devices: 34.7 us -> 44.1 us
  matrix products: 4.63 us -> 5.88 us
    all_gather x1 -> x0, blocking collectives: 13.9 us -> none  [body(): lax.all_gather(hidden, 'tp', axis=1, tiled=True)]
    ppermute x0 -> x7, starting transfers between devices: none -> 10.7 us  [the longest x3 10.4 us: start_patches(): upper = lax.ppermute(upper, 'tp', all_rows)]
    ppermute x0 -> x7, waiting for transfers between devices: none -> 10.1 us  [the longest x4 10.1 us: start_patches(): low = lax.ppermute(low, 'tp', by_rank)]
    dot_general x1 -> x8, matrix products: 0.45 us -> 1.7 us  [body(): jnp.einsum('ens,end->esd', own_block, lax.dynamic_slice_in_dim(w_down, st...]
  transfers between devices with their start and end apart: 2 -> 9, of which waited for: 2 -> 6; matrix products, arithmetic and copies ran while one was open for 0% -> 2% of each run, Pallas kernels for 0% -> 0%
where the time goes in v1:
time: 110 us
  waiting for transfers between devices  44.1 us (40%)
  blocking collectives  24.3 us (22%)
  starting transfers between devices  14.4 us (13%)
  between operations  13.8 us (13%)
  matrix products  5.88 us (5%)
  other arithmetic  3.86 us (4%)
  local copies, waits for them, and re-layouts  3.84 us (3%)
    all_gather x1, waiting for transfers between devices, body(): piece_cols = lax.all_gather(arrived, 'tp', axis=2, tiled=True)  28.8 us
    psum x1, blocking collectives, body(): square_total = lax.psum(jnp.sum(combined * combined, axis=1), 'tp')  13.6 us
    all_to_all x1, blocking collectives, body(): lax.all_to_all(outgoing, 'ep', split_axis=1, concat_axis=1, tiled=True)  10.7 us
    ppermute x3, starting transfers between devices, start_patches(): upper = lax.ppermute(upper, 'tp', all_rows)  10.4 us
    ppermute x4, waiting for transfers between devices, start_patches(): low = lax.ppermute(low, 'tp', by_rank)  10.1 us
    all_to_all x1, waiting for transfers between devices, body(): lax.all_to_all(expert_out.reshape(EXP_DEV, ep_count, slot_count, out_part...  5.25 us
    all_to_all x1, starting transfers between devices, body(): lax.all_to_all(expert_out.reshape(EXP_DEV, ep_count, slot_count, out_part...  3.65 us
    dot_general x1, matrix products, body(): jnp.einsum('efn,esn->efs', w_gate, piece_cols, preferred_element_type=jnp...  2.45 us
  transfers between devices with their start and end apart: 9, of which 6 were waited for; matrix products, arithmetic and copies ran while one was open for 2% of the time, Pallas kernels for 0%

profile of v1, /device:TPU:0, one launch (start us, length us, event | category | flops | bytes accessed | tf_op | source)
XLA Modules:
  0.0 110.2 jit_solution(17483547740056711763)
XLA Ops:
  6.5 0.0 copy-start
  6.5 0.0 all-gather.2.cloned.1.call-start
  6.5 0.9 copy.33
  7.5 0.1 eq.38
  7.6 0.1 fusion.20
  7.7 0.2 reduce_window_sum.11
  7.8 0.2 select_reduce_fusion
  8.0 0.1 reduce_sum.32
  8.1 0.1 copy.38
  8.2 0.1 fusion.19
  8.3 1.0 convolution_convert_fusion
  9.4 10.7 %all_to_all.10 = bf16[2,4,32,512]{3,2,0,1:T(8,128)(2,1)S(1)} all-to-all(bf16[2,4,32,512]{3,2,0,1:T(8,128)(2,1)S(1)} %copy.39), channel_id=1, replica_groups=mesh['ep'=4,'tp'=8] {'ep'}, dimensions={1} | all-to-all | bytes 524288 | tf_op jit(solution)/shard_map/all_to_all | solution.py:35
  20.1 0.7 copy.40
  20.8 0.0 all-gather.2.cloned.1.call-update
  21.0 0.1 reshape.182
  21.1 28.8 %all-gather.2.cloned.1.call-done = bf16[2,128,4096]{2,1,0:T(8,128)(2,1)} async-done(((bf16[2,128,512]{2,1,0:T(8,128)(2,1)}), bf16[2,128,4096]{2,1,0:T(8,128)(2,1)}) %all-gather.2.cloned.1.call-update) | async-done | bytes 2097168 | tf_op jit(solution)/shard_map/all_gather | solution.py:38
  49.9 0.0 copy-start.1
  49.9 2.2 %fusion = f32[2,128]{1,0:T(2,128)S(1)} fusion(bf16[2,128,4096]{2,1,0:T(8,128)(2,1)} %all-gather.2.cloned.1.call-done), kind=kLoop, calls=%fused_computation.2 | loop fusion | flops 3145472 | bytes 2098176 | tf_op jit(solution)/shard_map/esn,esn->es/dot_general | solution.py:41
  52.1 0.0 copy-done.1
  52.1 0.0 copy-start.4
  52.2 2.5 %fusion.6 = f32[2,128,128]{1,2,0:T(8,128)S(1)} fusion(bf16[2,128,4096]{2,1,0:T(8,128)(2,1)S(1)} %copy-done.1, bf16[2,128,4096]{2,1,0:T(8,128)(2,1)} %param.10, f32[2,128]{1,0:T(2,128)S(1)} %add_rsqrt_fusion), kind=kOutput, calls=%fused_computation.16 | convolution fusion | flops 268468224 | bytes 4326400 | tf_op jit(solution)/shard_map/efn,esn->efs/dot_general | solution.py:39
  54.6 0.0 copy-done.4
  54.6 0.7 fusion.7
  55.3 0.3 collective-permute-start.1
  55.6 3.3 %collective-permute-start = (bf16[2,128,128]{1,2,0:T(8,128)(2,1)S(1)}, bf16[2,128,128]{1,2,0:T(8,128)(2,1)S(1)}, u32[]{:S(2)}, u32[]{:S(2)}) collective-permute-start(bf16[2,128,128]{1,2,0:T(8,128)(2,1)S(1)} %fusion.7), channel_id=1, source_target_pairs={{0,7},{1,0},{2,1},{3,2},{4,3},{5,4},{6,5},{7,6},{8,15},{9,8},{10,9... | collective-permute-start | bytes 196616 | tf_op jit(solution)/shard_map/ppermute | solution.py:60
  58.9 0.0 copy-done
  58.9 0.2 fusion.17
  59.2 2.1 %collective-permute-done.1 = bf16[2,128,128]{1,2,0:T(8,128)(2,1)S(1)} collective-permute-done((bf16[2,128,128]{1,2,0:T(8,128)(2,1)S(1)}, bf16[2,128,128]{1,2,0:T(8,128)(2,1)S(1)}, u32[]{:S(2)}, u32[]{:S(2)}) %collective-permute-start.1) | collective-permute-done | bytes 65568 | tf_op jit(solution)/shard_map/ppermute | solution.py:58
  61.3 0.0 collective-permute-start.3
  61.3 0.0 collective-permute-done
  61.3 3.5 %collective-permute-start.2 = (bf16[2,128,128]{1,2,0:T(8,128)(2,1)S(1)}, bf16[2,128,128]{1,2,0:T(8,128)(2,1)S(1)}, u32[]{:S(2)}, u32[]{:S(2)}) collective-permute-start(bf16[2,128,128]{1,2,0:T(8,128)(2,1)S(1)} %collective-permute-done), channel_id=1, source_target_pairs={{0,7},{1,0},{2,1},{3,2},{4,3},{5,4},{6,5},{7,6},{8,15},{9,8},{10,9... | collective-permute-start | bytes 196616 | tf_op jit(solution)/shard_map/ppermute | solution.py:60
  64.8 0.2 convolution_add_fusion.4
  65.0 0.2 convolution_add_fusion.3
  65.3 1.5 %collective-permute-done.3 = bf16[2,128,128]{1,2,0:T(8,128)(2,1)S(1)} collective-permute-done((bf16[2,128,128]{1,2,0:T(8,128)(2,1)S(1)}, bf16[2,128,128]{1,2,0:T(8,128)(2,1)S(1)}, u32[]{:S(2)}, u32[]{:S(2)}) %collective-permute-start.3) | collective-permute-done | bytes 65568 | tf_op jit(solution)/shard_map/ppermute | solution.py:58
  66.8 0.0 collective-permute-start.5
  66.8 0.2 fusion.12
  67.0 0.0 collective-permute-done.2
  67.0 3.6 %collective-permute-start.4 = (bf16[2,128,128]{1,2,0:T(8,128)(2,1)S(1)}, bf16[2,128,128]{1,2,0:T(8,128)(2,1)S(1)}, u32[]{:S(2)}, u32[]{:S(2)}) collective-permute-start(bf16[2,128,128]{1,2,0:T(8,128)(2,1)S(1)} %collective-permute-done.2), channel_id=1, source_target_pairs={{0,7},{1,0},{2,1},{3,2},{4,3},{5,4},{6,5},{7,6},{8,15},{9,8},{10,9... | collective-permute-start | bytes 196616 | tf_op jit(solution)/shard_map/ppermute | solution.py:60
  70.6 0.2 fusion.2
  70.8 1.5 %collective-permute-done.5 = bf16[2,128,128]{1,2,0:T(8,128)(2,1)S(1)} collective-permute-done((bf16[2,128,128]{1,2,0:T(8,128)(2,1)S(1)}, bf16[2,128,128]{1,2,0:T(8,128)(2,1)S(1)}, u32[]{:S(2)}, u32[]{:S(2)}) %collective-permute-start.5) | collective-permute-done | bytes 65568 | tf_op jit(solution)/shard_map/ppermute | solution.py:58
  72.3 0.0 collective-permute-start.6
  72.3 0.2 fusion.9
  72.5 0.0 copy-start.2
  72.5 0.0 collective-permute-done.4
  72.5 0.2 fusion.1
  72.7 0.0 copy-start.3
  72.7 5.0 %collective-permute-done.6 = bf16[2,128,128]{1,2,0:T(8,128)(2,1)S(1)} collective-permute-done((bf16[2,128,128]{1,2,0:T(8,128)(2,1)S(1)}, bf16[2,128,128]{1,2,0:T(8,128)(2,1)S(1)}, u32[]{:S(2)}, u32[]{:S(2)}) %collective-permute-start.6) | collective-permute-done | bytes 65568 | tf_op jit(solution)/shard_map/ppermute | solution.py:58
  77.7 0.2 fusion.3
  78.0 0.7 copy.41
  78.7 3.6 %all-to-all-start.1 = ((bf16[2,4,32,512]{3,2,0,1:T(8,128)(2,1)}), bf16[2,4,32,512]{3,2,0,1:T(8,128)(2,1)S(1)}, u32[]{:S(2)}, u32[]{:S(2)}) async-start(bf16[2,4,32,512]{3,2,0,1:T(8,128)(2,1)} %copy.41), calls=%async_computation.1 | async-start | bytes 524288 | tf_op jit(solution)/shard_map/all_to_all | solution.py:76
  82.3 0.0 copy-done.2
  82.3 0.1 copy.44
  82.4 5.3 %all-to-all-done.1 = bf16[2,4,32,512]{3,2,0,1:T(8,128)(2,1)S(1)} async-done(((bf16[2,4,32,512]{3,2,0,1:T(8,128)(2,1)}), bf16[2,4,32,512]{3,2,0,1:T(8,128)(2,1)S(1)}, u32[]{:S(2)}, u32[]{:S(2)}) %all-to-all-start.1) | async-done | bytes 262176 | tf_op jit(solution)/shard_map/all_to_all | solution.py:76
  87.7 0.8 gather_fusion
  88.6 0.1 reshape.183
  88.7 0.2 multiply_reduce_fusion
  88.9 0.1 multiply_reduce_fusion.1
  89.0 13.6 %psum.7 = f32[32]{0:T(128)S(1)} all-reduce(f32[32]{0:T(128)S(1)} %multiply_reduce_fusion.1), channel_id=1, replica_groups=mesh['ep'=4,'tp'=8] {'tp'}, use_global_device_ids=true, to_apply=%region_5.6 | all-reduce | flops 32 | bytes 256 | tf_op jit(solution)/shard_map/psum | solution.py:86
  102.6 0.0 copy-done.3
  102.6 0.7 multiply_convert_fusion
  (7 shorter events, 0.1 us)
Async XLA Ops:
  6.5 52.4 %copy-start = (bf16[2,1024,512]{2,1,0:T(8,128)(2,1)S(1)}, bf16[2,1024,512]{2,1,0:T(8,128)(2,1)}, u32[]{:S(2)}) copy-start(bf16[2,1024,512]{2,1,0:T(8,128)(2,1)} %param.12) | copy-start | bytes 6291460
  6.5 43.4 %all-gather.2.cloned.1.call-start = ((), (), s32[]{:S(2)}) async-start(), calls=%async_computation.2 | async-start | bytes 2359296 | tf_op jit(solution)/shard_map/all_gather | solution.py:38
  49.9 2.2 %copy-start.1 = (bf16[2,128,4096]{2,1,0:T(8,128)(2,1)S(1)}, bf16[2,128,4096]{2,1,0:T(8,128)(2,1)}, u32[]{:S(2)}) copy-start(bf16[2,128,4096]{2,1,0:T(8,128)(2,1)} %all-gather.2.cloned.1.call-done) | copy-start | bytes 6291460
  52.1 2.5 %copy-start.4 = (bf16[2,128,4096]{2,1,0:T(8,128)(2,1)S(1)}, bf16[2,128,4096]{2,1,0:T(8,128)(2,1)}, u32[]{:S(2)}) copy-start(bf16[2,128,4096]{2,1,0:T(8,128)(2,1)} %param.11) | copy-start | bytes 6291460
  55.3 5.9 %collective-permute-start.1 = (bf16[2,128,128]{1,2,0:T(8,128)(2,1)S(1)}, bf16[2,128,128]{1,2,0:T(8,128)(2,1)S(1)}, u32[]{:S(2)}, u32[]{:S(2)}) collective-permute-start(bf16[2,128,128]{1,2,0:T(8,128)(2,1)S(1)} %fusion.7), channel_id=1, source_target_pairs={{0,1},{1,2},{2,3},{3,4},{4,5},{5,6},{6,7},{7,0},{8,9},{9,10},{10,1... | collective-permute-start | bytes 196616 | tf_op jit(solution)/shard_map/ppermute | solution.py:58
  55.6 5.7 %collective-permute-start = (bf16[2,128,128]{1,2,0:T(8,128)(2,1)S(1)}, bf16[2,128,128]{1,2,0:T(8,128)(2,1)S(1)}, u32[]{:S(2)}, u32[]{:S(2)}) collective-permute-start(bf16[2,128,128]{1,2,0:T(8,128)(2,1)S(1)} %fusion.7), channel_id=1, source_target_pairs={{0,7},{1,0},{2,1},{3,2},{4,3},{5,4},{6,5},{7,6},{8,15},{9,8},{10,9... | collective-permute-start | bytes 196616 | tf_op jit(solution)/shard_map/ppermute | solution.py:60
  61.3 5.5 %collective-permute-start.3 = (bf16[2,128,128]{1,2,0:T(8,128)(2,1)S(1)}, bf16[2,128,128]{1,2,0:T(8,128)(2,1)S(1)}, u32[]{:S(2)}, u32[]{:S(2)}) collective-permute-start(bf16[2,128,128]{1,2,0:T(8,128)(2,1)S(1)} %collective-permute-done.1), channel_id=1, source_target_pairs={{0,1},{1,2},{2,3},{3,4},{4,5},{5,6},{6,7},{7,0},{8,9},{9,10},{10,1... | collective-permute-start | bytes 196616 | tf_op jit(solution)/shard_map/ppermute | solution.py:58
  61.3 5.7 %collective-permute-start.2 = (bf16[2,128,128]{1,2,0:T(8,128)(2,1)S(1)}, bf16[2,128,128]{1,2,0:T(8,128)(2,1)S(1)}, u32[]{:S(2)}, u32[]{:S(2)}) collective-permute-start(bf16[2,128,128]{1,2,0:T(8,128)(2,1)S(1)} %collective-permute-done), channel_id=1, source_target_pairs={{0,7},{1,0},{2,1},{3,2},{4,3},{5,4},{6,5},{7,6},{8,15},{9,8},{10,9... | collective-permute-start | bytes 196616 | tf_op jit(solution)/shard_map/ppermute | solution.py:60
  66.8 5.5 %collective-permute-start.5 = (bf16[2,128,128]{1,2,0:T(8,128)(2,1)S(1)}, bf16[2,128,128]{1,2,0:T(8,128)(2,1)S(1)}, u32[]{:S(2)}, u32[]{:S(2)}) collective-permute-start(bf16[2,128,128]{1,2,0:T(8,128)(2,1)S(1)} %collective-permute-done.3), channel_id=1, source_target_pairs={{0,1},{1,2},{2,3},{3,4},{4,5},{5,6},{6,7},{7,0},{8,9},{9,10},{10,1... | collective-permute-start | bytes 196616 | tf_op jit(solution)/shard_map/ppermute | solution.py:58
  67.0 5.5 %collective-permute-start.4 = (bf16[2,128,128]{1,2,0:T(8,128)(2,1)S(1)}, bf16[2,128,128]{1,2,0:T(8,128)(2,1)S(1)}, u32[]{:S(2)}, u32[]{:S(2)}) collective-permute-start(bf16[2,128,128]{1,2,0:T(8,128)(2,1)S(1)} %collective-permute-done.2), channel_id=1, source_target_pairs={{0,7},{1,0},{2,1},{3,2},{4,3},{5,4},{6,5},{7,6},{8,15},{9,8},{10,9... | collective-permute-start | bytes 196616 | tf_op jit(solution)/shard_map/ppermute | solution.py:60
  72.3 5.5 %collective-permute-start.6 = (bf16[2,128,128]{1,2,0:T(8,128)(2,1)S(1)}, bf16[2,128,128]{1,2,0:T(8,128)(2,1)S(1)}, u32[]{:S(2)}, u32[]{:S(2)}) collective-permute-start(bf16[2,128,128]{1,2,0:T(8,128)(2,1)S(1)} %collective-permute-done.5), channel_id=1, source_target_pairs={{0,1},{1,2},{2,3},{3,4},{4,5},{5,6},{6,7},{7,0},{8,9},{9,10},{10,1... | collective-permute-start | bytes 196616 | tf_op jit(solution)/shard_map/ppermute | solution.py:58
  72.5 9.9 %copy-start.2 = (f32[32,4]{0,1:T(4,128)S(1)}, f32[32,4]{0,1:T(4,128)}, u32[]{:S(2)}) copy-start(f32[32,4]{0,1:T(4,128)} %param.9) | copy-start | bytes 1540
  72.7 29.9 %copy-start.3 = (f32[512]{0:T(512)S(1)}, f32[512]{0:T(512)}, u32[]{:S(2)}) copy-start(f32[512]{0:T(512)} %param.13) | copy-start | bytes 6148
  78.7 9.0 %all-to-all-start.1 = ((bf16[2,4,32,512]{3,2,0,1:T(8,128)(2,1)}), bf16[2,4,32,512]{3,2,0,1:T(8,128)(2,1)S(1)}, u32[]{:S(2)}, u32[]{:S(2)}) async-start(bf16[2,4,32,512]{3,2,0,1:T(8,128)(2,1)} %copy.41), calls=%async_computation.1 | async-start | bytes 524288 | tf_op jit(solution)/shard_map/all_to_all | solution.py:76
Sparse Core Ops, SparseCore 0:
  21.0 28.8 all-gather.1
